TPU v7x, 32 devices: a whole 2x2x4 slice. The times are simulated.
32 devices in a mesh: ep: 8 (over z, x), tp: 4 (over y, core).
Axes of the slice: x: 2, y: 2, z: 4, core: 2. Of those that a mesh axis runs over, the one named last changes fastest.
Arguments:
- tokens: bfloat16 [1024, 2048], P('ep'), may hold values from -6 to 6
- cotangent: bfloat16 [1024, 2048], P('ep'), may hold values from -1.5 to 1.5
- routes: int32 [1024, 2], P('ep'), may hold values from 0 to 3, all different within a row; in each aligned block of 128 rows (0 to 127, 128 to 255, ...) at most 96 rows name the same one
- router: bfloat16 [2048, 4], replicated, may hold values from -0.125 to 0.125
- w_gate: bfloat16 [8, 2048, 2048], P('ep', None, 'tp'), may hold values from -0.125 to 0.125
- w_up: bfloat16 [8, 2048, 2048], P('ep', None, 'tp'), may hold values from -0.125 to 0.125
- w_down: bfloat16 [8, 2048, 2048], P('ep', 'tp'), may hold values from -0.09375 to 0.09375
Outputs:
- token_grad: bfloat16 [1024, 2048], P('ep', 'tp')
- gate_grad: float32 [1024, 2], P('ep')
- grad_gate: bfloat16 [8, 2048, 2048], P('ep', None, 'tp')
- grad_up: bfloat16 [8, 2048, 2048], P('ep', None, 'tp')
- grad_down: bfloat16 [8, 2048, 2048], P('ep', 'tp')
- router_grad: float32 [2048, 4], P(('ep', 'tp'))
Inputs may be any that keep to these rules, and one draw needn't show every extreme that they name: `routes`: each row names 2 different experts. In the rows of one index of ep (aligned blocks of 128 rows) no expert is named by more than 96 rows, a bound that some block reaches.
All inputs are finite; a program needn't handle non-finite values.
Results may differ from a plain program's by a relative error of at most 0.018.
Values may be sent and summed in bfloat16 or wider, within the bound.
No kernel may reach another device: no remote copies, remote signals or barrier semaphores. Data moves between devices by JAX's collectives and lax.ppermute only.
A program may use at most 64 MiB of HBM per device.

v0:
```python
import jax
import jax.numpy as jnp
from jax import lax
from jax.sharding import PartitionSpec as P

BLOCKS = 2


def build_slots(block_routes, experts, capacity):
    flat_routes = block_routes.reshape(-1)
    labels = jnp.arange(experts, dtype=jnp.int32)
    hit_mask = (flat_routes[None, :] == labels[:, None]).astype(jnp.int32)
    rank_in = jnp.cumsum(hit_mask, axis=1, dtype=jnp.int32) - 1
    slot_ids = jnp.arange(capacity, dtype=jnp.int32)
    assigned = (hit_mask[:, None, :] == 1) & (rank_in[:, None, :] == slot_ids[None, :, None])
    return assigned.astype(jnp.float32)


def gate_pair(tokens, routes, router, experts):
    logits = jnp.dot(tokens, router, preferred_element_type=jnp.float32)
    labels = jnp.arange(experts, dtype=jnp.int32)
    picked = (routes[:, :, None] == labels[None, None, :]).astype(jnp.float32)
    chosen = jnp.sum(picked * logits[:, None, :], axis=2)
    margin = chosen[:, 0] - chosen[:, 1]
    weights = jnp.stack([jax.nn.sigmoid(margin), jax.nn.sigmoid(-margin)], axis=1)
    return (picked, weights)


def logit_grads(picked, weights, gate_grad):
    lead_grad = weights[:, 0] * weights[:, 1] * (gate_grad[:, 0] - gate_grad[:, 1])
    pair_grad = jnp.stack([lead_grad, -lead_grad], axis=1)
    return jnp.sum(picked * pair_grad[:, :, None], axis=1)


def expert_grads(rows_in, cot_in, gate_in, gate_weight, up_weight, down_weight):
    pre_gate = jnp.dot(rows_in, gate_weight, preferred_element_type=jnp.float32)
    pre_up = jnp.dot(rows_in, up_weight, preferred_element_type=jnp.float32)
    back_grad = lax.dot_general(
        cot_in, down_weight, (((1,), (1,)), ((), ())), preferred_element_type=jnp.float32
    )
    sig_gate = jax.nn.sigmoid(pre_gate)
    active = pre_gate * sig_gate
    hidden = (active * pre_up).astype(jnp.bfloat16)
    gate_terms = jnp.sum(hidden.astype(jnp.float32) * back_grad, axis=1)
    gate_col = gate_in.astype(jnp.float32)[:, None]
    scaled_back = gate_col * back_grad
    d_gate = (scaled_back * pre_up * sig_gate * (1.0 + pre_gate * (1.0 - sig_gate))).astype(
        jnp.bfloat16
    )
    d_up = (scaled_back * active).astype(jnp.bfloat16)
    scaled_cot = (gate_col * cot_in.astype(jnp.float32)).astype(jnp.bfloat16)
    contract_rows = (((0,), (0,)), ((), ()))
    grad_gate = lax.dot_general(
        rows_in, d_gate, contract_rows, preferred_element_type=jnp.float32
    ).astype(jnp.bfloat16)
    grad_up = lax.dot_general(
        rows_in, d_up, contract_rows, preferred_element_type=jnp.float32
    ).astype(jnp.bfloat16)
    grad_down = lax.dot_general(
        hidden, scaled_cot, contract_rows, preferred_element_type=jnp.float32
    ).astype(jnp.bfloat16)
    return (d_gate, d_up, gate_terms, grad_gate, grad_up, grad_down)


def spread_slabs(packed, experts, slab_count):
    widened = jnp.broadcast_to(packed[:, None], (experts, BLOCKS) + packed.shape[1:])
    return widened.reshape((slab_count,) + packed.shape[1:])


def shards(tokens, cotangent, routes, router, w_gate, w_up, w_down):
    highest = lax.Precision.HIGHEST
    ep_count = lax.axis_size("ep")
    tp_count = lax.axis_size("tp")
    experts = ep_count // BLOCKS
    tok_rows, width = tokens.shape
    top_count = routes.shape[1]
    capacity = 3 * tok_rows * top_count // (2 * experts)
    col_width = width // tp_count
    tp_index = lax.axis_index("tp")
    picked, weights = gate_pair(tokens, routes, router, experts)
    assigned = build_slots(routes, experts, capacity)
    per_token = jnp.sum(assigned.reshape(experts, capacity, tok_rows, top_count), axis=3)
    token_map = per_token.astype(jnp.bfloat16)
    gate_send = weights.astype(jnp.bfloat16)
    gate_slots = jnp.einsum(
        "ecj,j->ec", assigned, gate_send.astype(jnp.float32).reshape(-1), precision=highest
    ).astype(jnp.bfloat16)
    gate_out = spread_slabs(gate_slots, experts, ep_count)

    def pack_rows(source):
        packed = jnp.einsum(
            "ect,td->ecd", token_map, source, preferred_element_type=jnp.float32
        ).astype(jnp.bfloat16)
        return spread_slabs(packed, experts, ep_count)

    tok_part = lax.dynamic_slice_in_dim(tokens, tp_index * col_width, col_width, 1)
    cot_part = lax.dynamic_slice_in_dim(cotangent, tp_index * col_width, col_width, 1)
    recv_part, recv_cot_part, recv_gate = (
        lax.all_to_all(pack_rows(tok_part), "ep", split_axis=0, concat_axis=0, tiled=True),
        lax.all_to_all(pack_rows(cot_part), "ep", split_axis=0, concat_axis=0, tiled=True),
        lax.all_to_all(gate_out, "ep", split_axis=0, concat_axis=0, tiled=True),
    )
    recv_rows, recv_cot = (
        lax.all_gather(recv_part, "tp", axis=2, tiled=True),
        lax.all_gather(recv_cot_part, "tp", axis=2, tiled=True),
    )
    rows_in = recv_rows.reshape(-1, width)
    cot_in = recv_cot.reshape(-1, width)
    gate_in = recv_gate.reshape(-1)
    d_gate, d_up, gate_terms, grad_gate, grad_up, grad_down = expert_grads(
        rows_in, cot_in, gate_in, w_gate[0], w_up[0], w_down[0]
    )
    contract_hidden = (((1,), (1,)), ((), ()))
    partial_dx = lax.dot_general(
        d_gate, w_gate[0], contract_hidden, preferred_element_type=jnp.float32
    )
    partial_dx = partial_dx + lax.dot_general(
        d_up, w_up[0], contract_hidden, preferred_element_type=jnp.float32
    )
    summed_dx = lax.psum_scatter(
        partial_dx.reshape(ep_count, capacity, width).astype(jnp.bfloat16),
        "tp",
        scatter_dimension=2,
        tiled=True,
    ).astype(jnp.float32)
    gate_sums = lax.psum(gate_terms.reshape(ep_count, capacity), "tp")
    back_dx, back_gate = (
        lax.all_to_all(
            summed_dx.astype(jnp.bfloat16), "ep", split_axis=0, concat_axis=0, tiled=True
        ).astype(summed_dx.dtype),
        lax.all_to_all(
            gate_sums.astype(jnp.bfloat16), "ep", split_axis=0, concat_axis=0, tiled=True
        ).astype(gate_sums.dtype),
    )
    slab_dx = jnp.sum(back_dx.reshape(experts, BLOCKS, capacity, col_width), axis=1)
    routed_dx = jnp.einsum("ect,ecd->td", per_token, slab_dx, precision=highest)
    slab_gate = jnp.sum(back_gate.reshape(experts, BLOCKS, capacity), axis=1)
    gate_grad = jnp.einsum("ecj,ec->j", assigned, slab_gate, precision=highest).reshape(
        tok_rows, top_count
    )
    logit_grad = logit_grads(picked, weights, gate_grad)
    router_cols = lax.dynamic_slice_in_dim(router, tp_index * col_width, col_width, 0).astype(
        jnp.float32
    )
    token_grad = (routed_dx + jnp.dot(logit_grad, router_cols.T, precision=highest)).astype(
        jnp.bfloat16
    )
    seg_rows = tok_rows // tp_count
    own_rows = lax.dynamic_slice_in_dim(tokens, tp_index * seg_rows, seg_rows, 0).astype(
        jnp.float32
    )
    own_logit = lax.dynamic_slice_in_dim(logit_grad, tp_index * seg_rows, seg_rows, 0)
    router_grad = lax.psum_scatter(
        jnp.dot(own_rows.T, own_logit, precision=highest),
        ("ep", "tp"),
        scatter_dimension=0,
        tiled=True,
    )
    return (token_grad, gate_grad, grad_gate[None], grad_up[None], grad_down[None], router_grad)


def solution(mesh):
    placed = (
        P("ep", None),
        P("ep", None),
        P("ep", None),
        P(),
        P("ep", None, "tp"),
        P("ep", None, "tp"),
        P("ep", "tp", None),
    )
    return jax.shard_map(
        shards,
        mesh=mesh,
        in_specs=placed,
        out_specs=(
            P("ep", "tp"),
            P("ep", None),
            P("ep", None, "tp"),
            P("ep", None, "tp"),
            P("ep", "tp", None),
            P(("ep", "tp"), None),
        ),
        check_vma=False,
    )
```

profile of v0, /device:TPU:0, one launch (start us, length us, event | category | flops | bytes accessed | tf_op | source)
XLA Modules:
  0.0 325.1 jit_solution(1084350082928045645)
XLA Ops:
  8.3 1.2 reduce-window.6
  12.1 27.3 %all_to_all.33 = bf16[8,96,512]{2,1,0:T(8,128)(2,1)} all-to-all(bf16[8,96,512]{2,1,0:T(8,128)(2,1)S(1)} %bitcast.80), channel_id=1, replica_groups=mesh['ep'=8,'tp'=4] {'ep'}, dimensions={0} | all-to-all | bytes 1572864 | tf_op jit(solution)/shard_map/all_to_all | solution.py:99
  39.5 1.2 convolution_convert_fusion.3
  40.8 23.3 %all_to_all.34 = bf16[8,96,512]{2,1,0:T(8,128)(2,1)} all-to-all(bf16[8,96,512]{2,1,0:T(8,128)(2,1)S(1)} %bitcast.81), channel_id=1, replica_groups=mesh['ep'=8,'tp'=4] {'ep'}, dimensions={0} | all-to-all | bytes 1572864 | tf_op jit(solution)/shard_map/all_to_all | solution.py:100
  64.7 2.4 all-gather.5.cloned.1.call-done
  67.1 5.7 %fusion.11 = f32[768,512]{0,1:T(8,128)} fusion(bf16[768,2048]{1,0:T(8,128)(2,1)} %bitcast.95, bf16[1,2048,512]{2,1,0:T(8,128)(2,1)} %param.12), kind=kOutput, calls=%fused_computation.15 | convolution fusion | flops 1610612736 | bytes 6815744 | tf_op jit(solution)/shard_map/dot_general | solution.py:37
  72.8 3.0 fusion.8
  75.8 21.4 %all-gather.3.cloned.1.call-done = bf16[8,96,2048]{2,1,0:T(8,128)(2,1)} async-done(((bf16[8,96,512]{2,1,0:T(8,128)(2,1)}), bf16[8,96,2048]{2,1,0:T(8,128)(2,1)}) %all-gather.3.cloned.1.call-update) | async-done | bytes 3145744 | tf_op jit(solution)/shard_map/all_gather | solution.py:105
  97.2 6.7 %multiply_reduce_fusion = (f32[768]{0:T(1024)S(1)}, bf16[768,512]{0,1:T(8,128)(2,1)}, f32[768,512]{0,1:T(8,128)}) fusion(f32[768,512]{0,1:T(8,128)} %fusion.11, f32[768,512]{0,1:T(8,128)} %fusion.8, bf16[768,2048]{1,0:T(8,128)(2,1)} %bitcast.99, bf16[1,512,2048]{2,1,0:T(8,128)(2,1)} %param.13), kind=kOutput, calls=%fused_computation.20 | convolution fusion | flops 1614150912 | bytes 10750976 | tf_op jit(solution)/shard_map/dot_general | solution.py:38
  104.1 5.9 %psum.7 = bf16[8,96]{1,0:T(8,128)(2,1)S(1)} all-reduce(f32[8,96]{1,0:T(8,128)S(1)} %reshape.150), channel_id=1, replica_groups=mesh['ep'=8,'tp'=4] {'tp'}, use_global_device_ids=true, to_apply=%region_7.8 | all-reduce | flops 768 | bytes 4608 | tf_op jit(solution)/shard_map/psum | solution.py:126
  110.5 5.7 %all-to-all-start.4 = ((bf16[8,1,96]{2,1,0:T(2,128)(2,1)}), bf16[8,1,96]{2,1,0:T(2,128)(2,1)S(1)}, u32[]{:S(2)}, u32[]{:S(2)}) async-start(bf16[8,1,96]{2,1,0:T(2,128)(2,1)} %copy.80), calls=%async_computation.5 | async-start | bytes 8192 | tf_op jit(solution)/shard_map/all_to_all | solution.py:131
  116.5 6.1 %all-to-all-done.4 = bf16[8,1,96]{2,1,0:T(2,128)(2,1)S(1)} async-done(((bf16[8,1,96]{2,1,0:T(2,128)(2,1)}), bf16[8,1,96]{2,1,0:T(2,128)(2,1)S(1)}, u32[]{:S(2)}, u32[]{:S(2)}) %all-to-all-start.4) | async-done | bytes 1568 | tf_op jit(solution)/shard_map/all_to_all | solution.py:131
  123.4 8.9 %all_to_all.35 = bf16[8,1,96]{2,1,0:T(2,128)(2,1)S(1)} all-to-all(bf16[8,1,96]{2,1,0:T(2,128)(2,1)S(1)} %copy.77), channel_id=1, replica_groups=mesh['ep'=8,'tp'=4] {'ep'}, dimensions={0} | all-to-all | bytes 3072 | tf_op jit(solution)/shard_map/all_to_all | solution.py:101
  132.4 3.1 multiply_convert_fusion.7
  135.5 1.8 fusion.6
  137.7 3.5 %add_convert_fusion = bf16[768,2048]{1,0:T(8,128)(2,1)} fusion(f32[768,2048]{1,0:T(8,128)S(1)} %fusion.6, bf16[768,512]{0,1:T(8,128)(2,1)S(1)} %get-tuple-element.12, bf16[1,2048,512]{2,1,0:T(8,128)(2,1)S(1)} %copy-done.4), kind=kOutput, calls=%fused_computation.1 | convolution fusion | flops 1613758464 | bytes 12320768 | tf_op jit(solution)/shard_map/dot_general | solution.py:117
  141.4 1.8 fusion.31
  143.2 33.2 %reduce-scatter.5.cloned.1.call-done = bf16[8,96,512]{2,1,0:T(8,128)(2,1)} async-done(((bf16[8,96,2048]{2,1,0:T(8,128)(2,1)}), bf16[8,96,512]{2,1,0:T(8,128)(2,1)}) %reduce-scatter.5.cloned.1.call-update) | async-done | bytes 786448 | tf_op jit(solution)/shard_map/reduce_scatter | solution.py:120
  176.4 5.5 %all-to-all-start.3 = ((bf16[8,96,512]{2,1,0:T(8,128)(2,1)}), bf16[8,96,512]{2,1,0:T(8,128)(2,1)S(1)}, u32[]{:S(2)}, u32[]{:S(2)}) async-start(bf16[8,96,512]{2,1,0:T(8,128)(2,1)} %reduce-scatter.5.cloned.1.call-done), calls=%async_computation.4 | async-start | bytes 1572864 | tf_op jit(solution)/shard_map/all_to_all | solution.py:128
  181.9 5.4 %fusion.3 = bf16[1,2048,512]{2,1,0:T(8,128)(2,1)} fusion(bf16[768,2048]{1,0:T(8,128)(2,1)} %bitcast.96, bf16[768,512]{0,1:T(8,128)(2,1)} %copy-done.3), kind=kOutput, calls=%fused_computation.7 | convolution fusion | flops 1611661312 | bytes 6029312 | tf_op jit(solution)/shard_map/dot_general | solution.py:53
  187.3 3.2 fusion.5
  190.6 3.2 fusion.4
  193.8 121.5 %reduce-scatter.7.cloned.1.call-done = f32[64,4]{1,0:T(8,128)} async-done(((f32[2048,4]{1,0:T(8,128)}), f32[64,4]{1,0:T(8,128)}) %reduce-scatter.7.cloned.1.call-update) | async-done | bytes 1040
  315.3 1.4 copy.85
  (81 shorter events, 8.4 us)
Async XLA Ops:
  7.2 65.6 %copy-start = (bf16[1,2048,512]{2,1,0:T(8,128)(2,1)S(1)}, bf16[1,2048,512]{2,1,0:T(8,128)(2,1)}, u32[]{:S(2)}) copy-start(bf16[1,2048,512]{2,1,0:T(8,128)(2,1)} %param.11) | copy-start | bytes 6291460
  7.2 60.0 %all-gather.5.cloned.1.call-start = ((), (), s32[]{:S(2)}) async-start(), calls=%async_computation.8 | async-start | bytes 3932160 | tf_op jit(solution)/shard_map/all_gather | solution.py:104
  39.4 24.9 %copy-start.7 = (s32[128,2]{0,1:T(2,128)S(1)}, s32[128,2]{0,1:T(2,128)}, u32[]{:S(2)}) copy-start(s32[128,2]{0,1:T(2,128)} %param.9) | copy-start | bytes 3076
  39.5 25.0 %copy-start.5 = (bf16[128,2048]{1,0:T(8,128)(2,1)S(1)}, bf16[128,2048]{1,0:T(8,128)(2,1)}, u32[]{:S(2)}) copy-start(bf16[128,2048]{1,0:T(8,128)(2,1)} %param.7) | copy-start | bytes 1572868
  39.5 25.0 %copy-start.6 = (bf16[2048,4]{0,1:T(4,128)(2,1)S(1)}, bf16[2048,4]{0,1:T(4,128)(2,1)}, u32[]{:S(2)}) copy-start(bf16[2048,4]{0,1:T(4,128)(2,1)} %param.10) | copy-start | bytes 49156
  39.5 57.8 %all-gather.3.cloned.1.call-start = ((), (), s32[]{:S(2)}) async-start(), calls=%async_computation.7 | async-start | bytes 3932160 | tf_op jit(solution)/shard_map/all_gather | solution.py:105
  67.1 5.7 %copy-start.9 = (bf16[8,96,2048]{2,1,0:T(8,128)(2,1)S(1)}, bf16[8,96,2048]{2,1,0:T(8,128)(2,1)}, u32[]{:S(2)}) copy-start(bf16[8,96,2048]{2,1,0:T(8,128)(2,1)} %all-gather.5.cloned.1.call-done) | copy-start | bytes 9437188
  110.5 12.1 %all-to-all-start.4 = ((bf16[8,1,96]{2,1,0:T(2,128)(2,1)}), bf16[8,1,96]{2,1,0:T(2,128)(2,1)S(1)}, u32[]{:S(2)}, u32[]{:S(2)}) async-start(bf16[8,1,96]{2,1,0:T(2,128)(2,1)} %copy.80), calls=%async_computation.5 | async-start | bytes 8192 | tf_op jit(solution)/shard_map/all_to_all | solution.py:131
  116.2 60.2 %reduce-scatter.5.cloned.1.call-start = ((), (), s32[]{:S(2)}) async-start(), calls=%async_computation.9 | async-start | bytes 3932160 | tf_op jit(solution)/shard_map/reduce_scatter | solution.py:120
  122.8 12.7 %copy-start.8 = (f32[1,128,2,1]{1,0,3,2:T(1,128)}, f32[1,128,2,1]{1,0,3,2:T(1,128)S(1)}, u32[]{:S(2)}) copy-start(f32[1,128,2,1]{1,0,3,2:T(1,128)S(1)} %fusion.23) | copy-start | bytes 3076
  135.5 1.9 copy-start.3
  135.5 1.9 copy-start.1
  135.5 2.2 copy-start.4
  141.3 174.1 %reduce-scatter.7.cloned.1.call-start = ((), (), s32[]{:S(2)}) async-start(), calls=%async_computation.10 | async-start | bytes 1081344
  176.4 140.3 %all-to-all-start.3 = ((bf16[8,96,512]{2,1,0:T(8,128)(2,1)}), bf16[8,96,512]{2,1,0:T(8,128)(2,1)S(1)}, u32[]{:S(2)}, u32[]{:S(2)}) async-start(bf16[8,96,512]{2,1,0:T(8,128)(2,1)} %reduce-scatter.5.cloned.1.call-done), calls=%async_computation.4 | async-start | bytes 1572864 | tf_op jit(solution)/shard_map/all_to_all | solution.py:128
  181.9 5.4 %copy-start.11 = (bf16[8,96,2048]{2,1,0:T(8,128)(2,1)S(1)}, bf16[8,96,2048]{2,1,0:T(8,128)(2,1)}, u32[]{:S(2)}) copy-start(bf16[8,96,2048]{2,1,0:T(8,128)(2,1)} %all-gather.3.cloned.1.call-done) | copy-start | bytes 9437188
  181.9 5.4 %copy-start.12 = (bf16[768,512]{0,1:T(8,128)(2,1)S(1)}, bf16[768,512]{0,1:T(8,128)(2,1)}, u32[]{:S(2)}) copy-start(bf16[768,512]{0,1:T(8,128)(2,1)} %get-tuple-element.11) | copy-start | bytes 2359300
  187.3 3.3 %copy-start.2 = (bf16[768,512]{0,1:T(8,128)(2,1)S(1)}, bf16[768,512]{0,1:T(8,128)(2,1)}, u32[]{:S(2)}) copy-start(bf16[768,512]{0,1:T(8,128)(2,1)} %copy-done.1) | copy-start | bytes 2359300
  187.3 3.3 %copy-start.10 = (bf16[8,96,2048]{2,1,0:T(8,128)(2,1)S(1)}, bf16[8,96,2048]{2,1,0:T(8,128)(2,1)}, u32[]{:S(2)}) copy-start(bf16[8,96,2048]{2,1,0:T(8,128)(2,1)} %all-gather.5.cloned.1.call-done) | copy-start | bytes 9437188
Sparse Core Ops, SparseCore 0:
  39.6 27.5 all-gather.4
  68.7 28.4 all-gather.2
  141.4 34.9 reduce-scatter.4
  178.5 136.7 reduce-scatter.6
where the time goes:
time: 326 us; the launch traced here: 325 us
  waiting for transfers between devices  185 us (57%)
  blocking collectives  65.4 us (20%)
  matrix products  39.1 us (12%)
  between operations  14.1 us (4%)
  starting transfers between devices  11.3 us (3%)
  other arithmetic  5.65 us (2%)
  local copies, waits for them, and re-layouts  4.82 us (1%)
    unnamed x5, waiting for transfers between devices  122 us
    reduce_scatter x1, waiting for transfers between devices, shards(): lax.psum_scatter(partial_dx.reshape(ep_count, capacity, width).astype(jnp...  33.2 us
    all_to_all x1, blocking collectives, shards(): lax.all_to_all(pack_rows(tok_part), 'ep', split_axis=0, concat_axis=0, ti...  27.3 us
    all_to_all x1, blocking collectives, shards(): lax.all_to_all(pack_rows(cot_part), 'ep', split_axis=0, concat_axis=0, ti...  23.3 us
    all_gather x1, waiting for transfers between devices, shards(): lax.all_gather(recv_cot_part, 'tp', axis=2, tiled=True)  21.4 us
    all_to_all x1, blocking collectives, shards(): lax.all_to_all(gate_out, 'ep', split_axis=0, concat_axis=0, tiled=True)  8.86 us
    dot_general x1, matrix products, expert_grads(): lax.dot_general(cot_in, down_weight, (((1,), (1,)), ((), ())), preferred_...  6.74 us
  transfers between devices with their start and end apart: 6, of which 5 were waited for; matrix products, arithmetic and copies ran while one was open for 8% of the time, Pallas kernels for 0%

commit v1 on v0

--- a/solution.py
+++ b/solution.py
@@ -102,7 +102,9 @@
     )
     recv_rows, recv_cot = (
         lax.all_gather(recv_part, "tp", axis=2, tiled=True),
-        lax.all_gather(recv_cot_part, "tp", axis=2, tiled=True),
+        jnp.concatenate(
+            lax.all_to_all(jnp.stack([recv_cot_part] * lax.axis_size("tp")), "tp", 0, 0), axis=2
+        ),
     )
     rows_in = recv_rows.reshape(-1, width)
     cot_in = recv_cot.reshape(-1, width)

time: 326 us -> 345 us (1.058)
  waiting for transfers between devices: 185 us -> 197 us
  local copies, waits for them, and re-layouts: 4.82 us -> 15.7 us
  matrix products: 39.1 us -> 33.3 us
    all_to_all x0 -> x1, waiting for transfers between devices: none -> 36.4 us  [shards(): lax.all_to_all(jnp.stack([recv_cot_part] * lax.axis_size('tp')), 'tp', 0, 0)]
    all_gather x1 -> x0, waiting for transfers between devices: 21.4 us -> none  [shards(): lax.all_gather(recv_cot_part, 'tp', axis=2, tiled=True)]
    all_to_all x0 -> x1, starting transfers between devices: none -> 4.77 us  [shards(): lax.all_to_all(jnp.stack([recv_cot_part] * lax.axis_size('tp')), 'tp', 0, 0)]
    unnamed x29 -> x38, local copies, waits for them, and re-layouts: 2.68 us -> 7.18 us
    reshape x0 -> x1, local copies, waits for them, and re-layouts: none -> 4.32 us  [shards(): jnp.concatenate(lax.all_to_all(jnp.stack([recv_cot_part] * lax.axis_size(...]
    unnamed x5 -> x4, waiting for transfers between devices: 122 us -> 122 us
  transfers between devices with their start and end apart: 6 -> 6, of which waited for: 5 -> 4; matrix products, arithmetic and copies ran while one was open for 8% -> 8% of each run, Pallas kernels for 0% -> 0%
where the time goes in v1:
time: 345 us
  waiting for transfers between devices  197 us (57%)
  blocking collectives  65.1 us (19%)
  matrix products  33.3 us (10%)
  local copies, waits for them, and re-layouts  15.7 us (5%)
  starting transfers between devices  14.2 us (4%)
  between operations  14.1 us (4%)
  other arithmetic  5.65 us (2%)
    unnamed x4, waiting for transfers between devices  122 us
    all_to_all x1, waiting for transfers between devices, shards(): lax.all_to_all(jnp.stack([recv_cot_part] * lax.axis_size('tp')), 'tp', 0, 0)  36.4 us
    reduce_scatter x1, waiting for transfers between devices, shards(): lax.psum_scatter(partial_dx.reshape(ep_count, capacity, width).astype(jnp...  32.8 us
    all_to_all x1, blocking collectives, shards(): lax.all_to_all(pack_rows(tok_part), 'ep', split_axis=0, concat_axis=0, ti...  27.3 us
    all_to_all x1, blocking collectives, shards(): lax.all_to_all(pack_rows(cot_part), 'ep', split_axis=0, concat_axis=0, ti...  23.2 us
    all_to_all x1, blocking collectives, shards(): lax.all_to_all(gate_out, 'ep', split_axis=0, concat_axis=0, tiled=True)  8.86 us
    unnamed x38, local copies, waits for them, and re-layouts  7.18 us
  transfers between devices with their start and end apart: 6, of which 4 were waited for; matrix products, arithmetic and copies ran while one was open for 8% of the time, Pallas kernels for 0%

profile of v1, /device:TPU:0, one launch (start us, length us, event | category | flops | bytes accessed | tf_op | source)
XLA Modules:
  0.0 344.8 jit_solution(4844188904622592929)
XLA Ops:
  12.1 27.3 %all_to_all.38 = bf16[8,96,512]{2,1,0:T(8,128)(2,1)} all-to-all(bf16[8,96,512]{2,1,0:T(8,128)(2,1)S(1)} %bitcast.86), channel_id=1, replica_groups=mesh['ep'=8,'tp'=4] {'ep'}, dimensions={0} | all-to-all | bytes 1572864 | tf_op jit(solution)/shard_map/all_to_all | solution.py:99
  40.7 23.2 %all_to_all.39 = bf16[8,96,512]{2,1,0:T(8,128)(2,1)S(1)} all-to-all(bf16[8,96,512]{2,1,0:T(8,128)(2,1)S(1)} %bitcast.87), channel_id=1, replica_groups=mesh['ep'=8,'tp'=4] {'ep'}, dimensions={0} | all-to-all | bytes 1572864 | tf_op jit(solution)/shard_map/all_to_all | solution.py:100
  63.9 2.1 stack.8
  65.9 4.8 %all-to-all-start.2 = ((bf16[4,8,96,512]{3,2,1,0:T(8,128)(2,1)}), bf16[4,8,96,512]{3,2,1,0:T(8,128)(2,1)}, u32[]{:S(2)}, u32[]{:S(2)}) async-start(bf16[4,8,96,512]{3,2,1,0:T(8,128)(2,1)} %stack.8), calls=%async_computation.2 | async-start | bytes 6291456 | tf_op jit(solution)/shard_map/all_to_all | solution.py:106
  71.3 36.4 %all-to-all-done.2 = bf16[4,8,96,512]{3,2,1,0:T(8,128)(2,1)} async-done(((bf16[4,8,96,512]{3,2,1,0:T(8,128)(2,1)}), bf16[4,8,96,512]{3,2,1,0:T(8,128)(2,1)}, u32[]{:S(2)}, u32[]{:S(2)}) %all-to-all-start.2) | async-done | bytes 3145760 | tf_op jit(solution)/shard_map/all_to_all | solution.py:106
  107.7 4.3 %copy.81 = bf16[8,96,4,512]{3,2,1,0:T(4,128)(2,1)S(1)} copy(bf16[8,96,4,512]{3,1,0,2:T(8,128)(2,1)} %bitcast.8) | data formatting | bytes 6291456 | tf_op jit(solution)/shard_map/reshape | solution.py:105
  112.0 2.7 copy.91
  114.7 4.5 %fusion.11 = f32[768,512]{0,1:T(8,128)S(1)} fusion(bf16[768,2048]{1,0:T(8,128)(2,1)} %bitcast.101, bf16[1,2048,512]{2,1,0:T(8,128)(2,1)} %param.12), kind=kOutput, calls=%fused_computation.15 | convolution fusion | flops 1610612736 | bytes 6815744 | tf_op jit(solution)/shard_map/dot_general | solution.py:37
  119.3 1.8 fusion.8
  122.9 3.3 multiply_reduce_fusion
  126.3 5.7 %psum.7 = bf16[8,96]{1,0:T(8,128)(2,1)S(1)} all-reduce(f32[8,96]{1,0:T(8,128)S(1)} %reshape.152), channel_id=1, replica_groups=mesh['ep'=8,'tp'=4] {'tp'}, use_global_device_ids=true, to_apply=%region_7.8 | all-reduce | flops 768 | bytes 4608 | tf_op jit(solution)/shard_map/psum | solution.py:128
  132.7 3.6 %all-to-all-start.5 = ((bf16[8,1,96]{2,1,0:T(2,128)(2,1)}), bf16[8,1,96]{2,1,0:T(2,128)(2,1)S(1)}, u32[]{:S(2)}, u32[]{:S(2)}) async-start(bf16[8,1,96]{2,1,0:T(2,128)(2,1)} %copy.84), calls=%async_computation.6 | async-start | bytes 8192 | tf_op jit(solution)/shard_map/all_to_all | solution.py:133
  136.8 5.9 %all-to-all-done.5 = bf16[8,1,96]{2,1,0:T(2,128)(2,1)S(1)} async-done(((bf16[8,1,96]{2,1,0:T(2,128)(2,1)}), bf16[8,1,96]{2,1,0:T(2,128)(2,1)S(1)}, u32[]{:S(2)}, u32[]{:S(2)}) %all-to-all-start.5) | async-done | bytes 1568 | tf_op jit(solution)/shard_map/all_to_all | solution.py:133
  143.5 8.9 %all_to_all.40 = bf16[8,1,96]{2,1,0:T(2,128)(2,1)S(1)} all-to-all(bf16[8,1,96]{2,1,0:T(2,128)(2,1)S(1)} %copy.80), channel_id=1, replica_groups=mesh['ep'=8,'tp'=4] {'ep'}, dimensions={0} | all-to-all | bytes 3072 | tf_op jit(solution)/shard_map/all_to_all | solution.py:101
  152.5 3.1 multiply_convert_fusion.7
  155.7 1.8 fusion.6
  157.8 3.5 %add_convert_fusion = bf16[768,2048]{1,0:T(8,128)(2,1)} fusion(f32[768,2048]{1,0:T(8,128)S(1)} %fusion.6, bf16[768,512]{0,1:T(8,128)(2,1)S(1)} %get-tuple-element.12, bf16[1,2048,512]{2,1,0:T(8,128)(2,1)S(1)} %copy-done.6), kind=kOutput, calls=%fused_computation.1 | convolution fusion | flops 1613758464 | bytes 12320768 | tf_op jit(solution)/shard_map/dot_general | solution.py:119
  161.5 1.8 fusion.31
  163.3 32.8 %reduce-scatter.5.cloned.1.call-done = bf16[8,96,512]{2,1,0:T(8,128)(2,1)} async-done(((bf16[8,96,2048]{2,1,0:T(8,128)(2,1)}), bf16[8,96,512]{2,1,0:T(8,128)(2,1)}) %reduce-scatter.5.cloned.1.call-update) | async-done | bytes 786448 | tf_op jit(solution)/shard_map/reduce_scatter | solution.py:122
  196.1 5.5 %all-to-all-start.4 = ((bf16[8,96,512]{2,1,0:T(8,128)(2,1)}), bf16[8,96,512]{2,1,0:T(8,128)(2,1)S(1)}, u32[]{:S(2)}, u32[]{:S(2)}) async-start(bf16[8,96,512]{2,1,0:T(8,128)(2,1)} %reduce-scatter.5.cloned.1.call-done), calls=%async_computation.5 | async-start | bytes 1572864 | tf_op jit(solution)/shard_map/all_to_all | solution.py:130
  201.6 5.4 %fusion.3 = bf16[1,2048,512]{2,1,0:T(8,128)(2,1)} fusion(bf16[768,2048]{1,0:T(8,128)(2,1)} %bitcast.102, bf16[768,512]{0,1:T(8,128)(2,1)} %copy-done.5), kind=kOutput, calls=%fused_computation.7 | convolution fusion | flops 1611661312 | bytes 6029312 | tf_op jit(solution)/shard_map/dot_general | solution.py:53
  207.0 3.2 fusion.5
  210.3 3.2 fusion.4
  213.5 121.5 %reduce-scatter.7.cloned.1.call-done = f32[64,4]{1,0:T(8,128)} async-done(((f32[2048,4]{1,0:T(8,128)}), f32[64,4]{1,0:T(8,128)}) %reduce-scatter.7.cloned.1.call-update) | async-done | bytes 1040
  (91 shorter events, 14.1 us)
Async XLA Ops:
  7.2 112.1 %copy-start = (bf16[1,2048,512]{2,1,0:T(8,128)(2,1)S(1)}, bf16[1,2048,512]{2,1,0:T(8,128)(2,1)}, u32[]{:S(2)}) copy-start(bf16[1,2048,512]{2,1,0:T(8,128)(2,1)} %param.11) | copy-start | bytes 6291460
  7.2 107.5 %all-gather.2.cloned.1.call-start = ((), (), s32[]{:S(2)}) async-start(), calls=%async_computation.8 | async-start | bytes 3932160 | tf_op jit(solution)/shard_map/all_gather | solution.py:104
  65.9 5.0 %copy-start.11 = (s32[128,2]{0,1:T(2,128)S(1)}, s32[128,2]{0,1:T(2,128)}, u32[]{:S(2)}) copy-start(s32[128,2]{0,1:T(2,128)} %param.9) | copy-start | bytes 3076
  65.9 5.1 %copy-start.9 = (bf16[128,2048]{1,0:T(8,128)(2,1)S(1)}, bf16[128,2048]{1,0:T(8,128)(2,1)}, u32[]{:S(2)}) copy-start(bf16[128,2048]{1,0:T(8,128)(2,1)} %param.7) | copy-start | bytes 1572868
  65.9 5.1 %copy-start.10 = (bf16[2048,4]{0,1:T(4,128)(2,1)S(1)}, bf16[2048,4]{0,1:T(4,128)(2,1)}, u32[]{:S(2)}) copy-start(bf16[2048,4]{0,1:T(4,128)(2,1)} %param.10) | copy-start | bytes 49156
  65.9 41.7 %all-to-all-start.2 = ((bf16[4,8,96,512]{3,2,1,0:T(8,128)(2,1)}), bf16[4,8,96,512]{3,2,1,0:T(8,128)(2,1)}, u32[]{:S(2)}, u32[]{:S(2)}) async-start(bf16[4,8,96,512]{3,2,1,0:T(8,128)(2,1)} %stack.8), calls=%async_computation.2 | async-start | bytes 6291456 | tf_op jit(solution)/shard_map/all_to_all | solution.py:106
  114.7 4.5 %copy-start.13 = (bf16[8,96,2048]{2,1,0:T(8,128)(2,1)S(1)}, bf16[8,96,2048]{2,1,0:T(8,128)(2,1)}, u32[]{:S(2)}) copy-start(bf16[8,96,2048]{2,1,0:T(8,128)(2,1)} %all-gather.2.cloned.1.call-done) | copy-start | bytes 9437188
  119.2 1.9 copy-start.7
  119.3 2.5 copy-start.1
  119.3 3.7 %copy-start.15 = (bf16[1,512,2048]{2,1,0:T(8,128)(2,1)S(1)}, bf16[1,512,2048]{2,1,0:T(8,128)(2,1)}, u32[]{:S(2)}) copy-start(bf16[1,512,2048]{2,1,0:T(8,128)(2,1)} %param.13) | copy-start | bytes 6291460
  121.1 5.1 %copy-start.8 = (f32[768,512]{0,1:T(8,128)}, f32[768,512]{0,1:T(8,128)S(1)}, u32[]{:S(2)}) copy-start(f32[768,512]{0,1:T(8,128)S(1)} %fusion.8) | copy-start | bytes 4718596
  132.7 10.0 %all-to-all-start.5 = ((bf16[8,1,96]{2,1,0:T(2,128)(2,1)}), bf16[8,1,96]{2,1,0:T(2,128)(2,1)S(1)}, u32[]{:S(2)}, u32[]{:S(2)}) async-start(bf16[8,1,96]{2,1,0:T(2,128)(2,1)} %copy.84), calls=%async_computation.6 | async-start | bytes 8192 | tf_op jit(solution)/shard_map/all_to_all | solution.py:133
  136.3 59.8 %reduce-scatter.5.cloned.1.call-start = ((), (), s32[]{:S(2)}) async-start(), calls=%async_computation.9 | async-start | bytes 3932160 | tf_op jit(solution)/shard_map/reduce_scatter | solution.py:122
  142.9 12.7 %copy-start.12 = (f32[1,128,2,1]{1,0,3,2:T(1,128)}, f32[1,128,2,1]{1,0,3,2:T(1,128)S(1)}, u32[]{:S(2)}) copy-start(f32[1,128,2,1]{1,0,3,2:T(1,128)S(1)} %fusion.23) | copy-start | bytes 3076
  155.6 1.9 copy-start.5
  155.6 1.9 copy-start.3
  155.7 2.2 copy-start.6
  161.4 173.7 %reduce-scatter.7.cloned.1.call-start = ((), (), s32[]{:S(2)}) async-start(), calls=%async_computation.10 | async-start | bytes 1081344
  196.1 140.4 %all-to-all-start.4 = ((bf16[8,96,512]{2,1,0:T(8,128)(2,1)}), bf16[8,96,512]{2,1,0:T(8,128)(2,1)S(1)}, u32[]{:S(2)}, u32[]{:S(2)}) async-start(bf16[8,96,512]{2,1,0:T(8,128)(2,1)} %reduce-scatter.5.cloned.1.call-done), calls=%async_computation.5 | async-start | bytes 1572864 | tf_op jit(solution)/shard_map/all_to_all | solution.py:130
  201.6 5.4 %copy-start.2 = (bf16[96,8,4,512]{3,1,2,0:T(8,128)(2,1)S(1)}, bf16[96,8,4,512]{3,1,2,0:T(8,128)(2,1)}, u32[]{:S(2)}) copy-start(bf16[96,8,4,512]{3,1,2,0:T(8,128)(2,1)} %copy.91) | copy-start | bytes 9437188
  201.6 5.4 %copy-start.16 = (bf16[768,512]{0,1:T(8,128)(2,1)S(1)}, bf16[768,512]{0,1:T(8,128)(2,1)}, u32[]{:S(2)}) copy-start(bf16[768,512]{0,1:T(8,128)(2,1)} %get-tuple-element.11) | copy-start | bytes 2359300
  207.0 3.3 copy-start.4
  207.0 3.3 copy-start.14
Sparse Core Ops, SparseCore 0:
  39.6 27.5 all-gather.1
  161.5 34.5 reduce-scatter.4
  198.3 136.6 reduce-scatter.6
